TPU v7x, 32 devices: a whole 2x2x4 slice. The times are simulated.
32 devices in a mesh: sp: 8 (over z, x), tp: 4 (over y, core).
Axes of the slice: x: 2, y: 2, z: 4, core: 2. Of those that a mesh axis runs over, the one named last changes fastest.
Arguments:
- residual_in: bfloat16 [2048, 2048], P(('sp', 'tp')), may hold values from -6 to 6
- queries: bfloat16 [2048, 512], P('sp', 'tp'), may hold values from -6 to 6
- key_rows: bfloat16 [2048, 512], P('sp', 'tp'), may hold values from -6 to 6
- value_rows: bfloat16 [2048, 1024], P('sp', 'tp'), may hold values from -6 to 6
- out_gate: bfloat16 [2048, 1024], P('sp', 'tp'), may hold values from -6 to 6
- decay_logit: float32 [2048, 512], P('sp', 'tp'), may hold values from -30 to 30
- head_gain: bfloat16 [128], replicated, may hold values from 0.099609375 to 1.8984375
- w_out: bfloat16 [1024, 2048], replicated, may hold values from -0.1875 to 0.1875
- ffn_gain: bfloat16 [2048], replicated, may hold values from 0.099609375 to 1.8984375
- routing: int32 [2048, 4], P('sp'), may hold values from 0 to 7, all different within a row; in each aligned block of 64 rows (0 to 63, 64 to 127, ...) at most 64 rows name the same one
- route_weight: float32 [2048, 4], P(('sp', 'tp')), may hold values from 0.05 to 0.6
- w_gate: bfloat16 [8, 2048, 2048], P('sp', None, 'tp'), may hold values from -4 to 4
- w_up: bfloat16 [8, 2048, 2048], P('sp', None, 'tp'), may hold values from -4 to 4
- w_down: bfloat16 [8, 2048, 2048], P('sp', 'tp'), may hold values from -0.125 to 0.125
Outputs:
- layer_out: bfloat16 [2048, 2048], P(('sp', 'tp'))
Inputs may be any that keep to these rules, and one draw needn't show every extreme that they name: `routing`: each row names 4 different experts. In each aligned block of 64 rows no expert is named more than 64 times, a bound that some blocks reach.
All inputs are finite; a program needn't handle non-finite values.
Results may differ from a plain program's by a relative error of at most 0.03.
Values may be sent and summed in bfloat16 or wider, within the bound.
A program may use at most 128 MiB of HBM per device.

v0:
```python
import jax
import jax.numpy as jnp
from jax import lax
from jax.experimental import pallas as pl
from jax.experimental.pallas import tpu as pltpu
from jax.sharding import PartitionSpec as P
import functools

DK = 64
DV = 128


DECAY_TEMP = 16.0
CLAMP_LIMIT = 7.0
SIGMOID_SLOPE = 1.702
NORM_EPS = 1e-06
EXACT_PRECISION = lax.Precision.HIGHEST


def clamped_unit(gate_pre, up_pre):
    gate_cut = jnp.minimum(gate_pre, CLAMP_LIMIT)
    up_cut = jnp.clip(up_pre, -CLAMP_LIMIT, CLAMP_LIMIT)
    return (up_cut + 1.0) * (gate_cut * jax.nn.sigmoid(SIGMOID_SLOPE * gate_cut))


MESH = pl.DeviceIdType.MESH
LANES = 128
SUB = 32
EXP_CAP = 64.0


def nt_dot(left, right):
    return lax.dot_general(
        left, right, (((1,), (1,)), ((), ())), preferred_element_type=jnp.float32
    )


def tn_dot(left, right):
    return lax.dot_general(
        left, right, (((0,), (0,)), ((), ())), preferred_element_type=jnp.float32
    )


def mix_kernel(
    sp_count, tp_count,
    q_ref, k_ref, v_ref, gate_ref, decay_ref, head_gain_ref, w_hbm, ffn_gain_ref,
    routing_ref, weight_ref, res_in_ref,
    res_ref, ext_ref,
    states, attended, mixed, mixed_in, w_vmem,
    w_sem, state_send, state_recv, mix_send, mix_recv,
):
    sp_me, tp_me = lax.axis_index("sp"), lax.axis_index("tp")
    barrier = pltpu.get_barrier_semaphore()

    @pl.loop(1, sp_count)
    def _(d):
        pl.semaphore_signal(
            barrier, inc=1, device_id={"sp": lax.rem(sp_me + d, sp_count)}, device_id_type=MESH
        )

    @pl.loop(1, tp_count)
    def _(d):
        pl.semaphore_signal(
            barrier, inc=1, device_id={"tp": lax.rem(tp_me + d, tp_count)}, device_id_type=MESH
        )

    w_copy = pltpu.make_async_copy(w_hbm, w_vmem, w_sem)
    w_copy.start()

    tokens, key_lanes = q_ref.shape
    value_lanes = v_ref.shape[1]
    head_count = key_lanes // DK
    lane_head = lax.broadcasted_iota(jnp.int32, (1, key_lanes), 1) // DK
    logit = decay_ref[...]
    log_decay = (jnp.minimum(logit, 0.0) - jnp.log1p(jnp.exp(-jnp.abs(logit)))) / DECAY_TEMP
    row_id = lax.broadcasted_iota(jnp.int32, (tokens, tokens), 0)
    col_id = lax.broadcasted_iota(jnp.int32, (tokens, tokens), 1)
    lower = (row_id >= col_id).astype(jnp.float32)
    cumulative = jnp.dot(
        lower, log_decay, precision=EXACT_PRECISION, preferred_element_type=jnp.float32
    )
    keys = k_ref[...].astype(jnp.float32)
    query = q_ref[...].astype(jnp.float32) * DK ** (-0.5)
    values = v_ref[...]
    ending = cumulative[tokens - 1 :, :]
    wide = tn_dot(values, (keys * jnp.exp(ending - cumulative)).astype(jnp.bfloat16))
    state = jnp.zeros((DV, key_lanes), jnp.float32)
    for h in range(head_count):
        state = jnp.where(lane_head == h, wide[h * DV : (h + 1) * DV, :], state)
    passing = jnp.exp(ending)
    passing_hi = passing.astype(jnp.bfloat16).astype(jnp.float32)
    tail_row = lax.broadcasted_iota(jnp.int32, (16, key_lanes), 0)
    tail = jnp.where(
        tail_row == 0, passing_hi, jnp.where(tail_row == 1, passing - passing_hi, 0.0)
    )
    states[sp_me, 0:DV, :] = state.astype(jnp.bfloat16)
    states[sp_me, DV : DV + 16, :] = tail.astype(jnp.bfloat16)

    pl.semaphore_wait(barrier, sp_count + tp_count - 2)

    def state_copy(slot, d):
        return pltpu.make_async_remote_copy(
            src_ref=states.at[slot],
            dst_ref=states.at[slot],
            send_sem=state_send.at[d],
            recv_sem=state_recv.at[slot],
            device_id={"sp": lax.rem(sp_me + d, sp_count)},
            device_id_type=MESH,
        )

    @pl.loop(1, sp_count)
    def _(d):
        state_copy(sp_me, d).start()

    for i in range(tokens // SUB):
        first = i * SUB
        reach = min(-(-(first + SUB) // LANES) * LANES, tokens)
        start = cumulative[first - 1 : first, :] if i else jnp.zeros((1, key_lanes), jnp.float32)
        q_sub = query[first : first + SUB] * jnp.exp(cumulative[first : first + SUB] - start)
        k_sub = keys[:reach] * jnp.exp(jnp.minimum(start - cumulative[:reach], EXP_CAP))
        stacked = jnp.concatenate(
            [jnp.where(lane_head == h, q_sub, 0.0) for h in range(head_count)], axis=0
        )
        scores = nt_dot(stacked.astype(jnp.bfloat16), k_sub.astype(jnp.bfloat16))
        at_row = lax.broadcasted_iota(jnp.int32, scores.shape, 0) % SUB + first
        at_col = lax.broadcasted_iota(jnp.int32, scores.shape, 1)
        scores = jnp.where(at_row >= at_col, scores, 0.0).astype(jnp.bfloat16)
        inner = jnp.dot(scores, values[:reach], preferred_element_type=jnp.float32)
        for h in range(head_count):
            attended[first : first + SUB, h * DV : (h + 1) * DV] = inner[
                h * SUB : (h + 1) * SUB, h * DV : (h + 1) * DV
            ]

    @pl.loop(1, sp_count)
    def _(d):
        state_copy(lax.rem(sp_me + d, sp_count), d).wait_recv()

    def absorb(j, incoming):
        decay = states[j, DV : DV + 16, :].astype(jnp.float32)
        total = decay[0:1, :] + decay[1:2, :]
        following = total * incoming + states[j, 0:DV, :].astype(jnp.float32)
        return jnp.where(j < sp_me, following, incoming)

    incoming = lax.fori_loop(
        0, sp_count, absorb, jnp.zeros((DV, key_lanes), jnp.float32)
    ).astype(jnp.bfloat16)
    query_dec = query * jnp.exp(cumulative)
    for h in range(head_count):
        cols = slice(h * DV, (h + 1) * DV)
        readout = nt_dot(jnp.where(lane_head == h, query_dec, 0.0).astype(jnp.bfloat16), incoming)
        head = attended[:, cols] + readout
        scale = lax.rsqrt(jnp.mean(head * head, axis=-1, keepdims=True) + NORM_EPS)
        opened = gate_ref[:, cols].astype(jnp.float32)
        opened = opened * jax.nn.sigmoid(opened)
        mixed[:, cols] = (head * scale * head_gain_ref[...].astype(jnp.float32) * opened).astype(
            jnp.bfloat16
        )

    rows = res_in_ref.shape[0]

    def mix_copy(block, slot, d):
        return pltpu.make_async_remote_copy(
            src_ref=mixed.at[pl.ds(pl.multiple_of(block * rows, rows), rows)],
            dst_ref=mixed_in.at[slot],
            send_sem=mix_send.at[d],
            recv_sem=mix_recv.at[slot],
            device_id={"tp": lax.rem(tp_me + d, tp_count)},
            device_id_type=MESH,
        )

    for d in range(1, tp_count):
        mix_copy(lax.rem(tp_me + d, tp_count), tp_me, d).start()

    lane = lax.broadcasted_iota(jnp.int32, (rows, LANES), 1)
    named = routing_ref[pl.ds(pl.multiple_of(tp_me * rows, rows), rows), :]
    share = jnp.zeros((rows, LANES), jnp.float32)
    for j in range(weight_ref.shape[1]):
        share = share + jnp.where(
            lane % (LANES // 2) == named[:, j : j + 1], weight_ref[:, j : j + 1], 0.0
        )
    share_hi = share.astype(jnp.bfloat16).astype(jnp.float32)
    width = res_in_ref.shape[1]
    ext_ref[:, width:] = jnp.where(lane < LANES // 2, share_hi, share - share_hi).astype(
        jnp.bfloat16
    )

    w_copy.wait()

    def w_rows(j):
        return w_vmem[pl.ds(pl.multiple_of(j * value_lanes, value_lanes), value_lanes), :]

    projected = jnp.dot(
        mixed[pl.ds(pl.multiple_of(tp_me * rows, rows), rows), :],
        w_rows(tp_me),
        preferred_element_type=jnp.float32,
    )
    for d in range(1, tp_count):
        slot = lax.rem(tp_me + d, tp_count)
        mix_copy(slot, slot, d).wait_recv()
        projected = projected + jnp.dot(
            mixed_in[slot], w_rows(slot), preferred_element_type=jnp.float32
        )
    residual = (res_in_ref[...].astype(jnp.float32) + projected).astype(jnp.bfloat16)
    res_ref[...] = residual
    wide_res = residual.astype(jnp.float32)
    inv = lax.rsqrt(jnp.mean(wide_res * wide_res, axis=-1, keepdims=True) + NORM_EPS)
    ext_ref[:, :width] = (wide_res * inv * ffn_gain_ref[...].astype(jnp.float32)).astype(
        jnp.bfloat16
    )

    @pl.loop(1, sp_count)
    def _(d):
        state_copy(sp_me, d).wait_send()

    for d in range(1, tp_count):
        mix_copy(lax.rem(tp_me + d, tp_count), tp_me, d).wait_send()


def mix_rows(
    queries, key_rows, value_rows, out_gate, decay_logit, head_gain, w_out,
    ffn_gain, routing, route_weight, residual_in,
):
    sp_count, tp_count = lax.axis_size("sp"), lax.axis_size("tp")
    rows, width = residual_in.shape
    tokens, key_lanes = queries.shape
    value_lanes = value_rows.shape[1]
    vmem = pl.BlockSpec(memory_space=pltpu.VMEM)
    return pl.pallas_call(
        functools.partial(mix_kernel, sp_count, tp_count),
        out_shape=(
            jax.ShapeDtypeStruct((rows, width), jnp.bfloat16),
            jax.ShapeDtypeStruct((rows, width + LANES), jnp.bfloat16),
        ),
        in_specs=[vmem] * 6 + [pl.BlockSpec(memory_space=pl.ANY)] + [vmem] * 4,
        out_specs=(vmem, vmem),
        scratch_shapes=[
            pltpu.VMEM((sp_count, DV + 16, key_lanes), jnp.bfloat16),
            pltpu.VMEM((tokens, value_lanes), jnp.float32),
            pltpu.VMEM((tokens, value_lanes), jnp.bfloat16),
            pltpu.VMEM((tp_count, rows, value_lanes), jnp.bfloat16),
            pltpu.VMEM(w_out.shape, jnp.bfloat16),
            pltpu.SemaphoreType.DMA,
            pltpu.SemaphoreType.DMA((sp_count,)),
            pltpu.SemaphoreType.DMA((sp_count,)),
            pltpu.SemaphoreType.DMA((tp_count,)),
            pltpu.SemaphoreType.DMA((tp_count,)),
        ],
        compiler_params=pltpu.CompilerParams(
            collective_id=0, has_side_effects=True, vmem_limit_bytes=40 << 20
        ),
        name="mix_rows",
    )(
        queries, key_rows, value_rows, out_gate, decay_logit, head_gain.reshape(1, -1), w_out,
        ffn_gain.reshape(1, -1), routing, route_weight, residual_in,
    )


def expert_kernel(
    z_count, y_count, gather_cuts, reduce_cuts,
    ext_ref, res_ref, gate_hbm, up_hbm, down_hbm, out_ref,
    rows_all, gate_w, up_w, down_w, hidden, shares, parts, got_core, got_first, got_second, got_z,
    w_sem, own_sem, gather_send, gather_recv, reduce_send, reduce_recv,
):
    sp_me, tp_me = lax.axis_index("sp"), lax.axis_index("tp")
    z, x = sp_me // 2, lax.rem(sp_me, 2)
    y, c = tp_me // 2, lax.rem(tp_me, 2)
    partner = {
        "x": {"sp": z * 2 + 1 - x},
        "y": {"tp": (1 - y) * 2 + c},
        "c": {"tp": y * 2 + 1 - c},
    }
    barrier = pltpu.get_barrier_semaphore()

    def z_peer(d):
        return {"sp": lax.rem(z + d, z_count) * 2 + x}

    for target in [z_peer(d) for d in range(1, z_count)] + list(partner.values()):
        pl.semaphore_signal(barrier, inc=1, device_id=target, device_id_type=MESH)
    loads = [
        pltpu.make_async_copy(src, dst, w_sem.at[i])
        for i, (src, dst) in enumerate(((gate_hbm, gate_w), (up_hbm, up_w), (down_hbm, down_w)))
    ]
    own = pltpu.make_async_copy(ext_ref, rows_all.at[z, x, y, c], own_sem)
    own.start()
    for load in loads:
        load.start()
    own.wait()
    pl.semaphore_wait(barrier, z_count + 2)

    def remote(src, dst, send, recv, target):
        return pltpu.make_async_remote_copy(
            src_ref=src, dst_ref=dst, send_sem=send, recv_sem=recv,
            device_id=target, device_id_type=MESH,
        )

    def gather_copies(i, stage, arriving):
        cols = pl.ds(gather_cuts[i][0], gather_cuts[i][1])
        order = ("x", "y") if i % 2 else ("y", "x")
        if stage == 0:
            copies = []
            for d in range(1, z_count):
                zz = lax.rem(z + z_count - d, z_count) if arriving else z
                block = rows_all.at[zz, x, y, c, :, cols]
                copies.append(
                    remote(block, block, gather_send.at[i, d], gather_recv.at[i, d], z_peer(d))
                )
            return copies
        axis = order[stage - 1] if stage < 3 else "c"
        xx = 1 - x if arriving and axis == "x" else x
        yy = 1 - y if arriving and axis == "y" else y
        cc = 1 - c if arriving and axis == "c" else c
        if stage == 1:
            block = rows_all.at[:, xx, yy, cc, :, cols]
        elif stage == 2 and axis == "x":
            block = rows_all.at[:, xx, :, cc, :, cols]
        elif stage == 2:
            block = rows_all.at[:, :, yy, cc, :, cols]
        else:
            block = rows_all.at[:, :, :, cc, :, cols]
        sem = z_count - 1 + stage
        return [
            remote(block, block, gather_send.at[i, sem], gather_recv.at[i, sem], partner[axis])
        ]

    chunks = len(gather_cuts)
    for tick in range(chunks // 2 + 4):
        for i in range(chunks):
            stage = tick - i // 2
            if 1 <= stage <= 4:
                for copy in gather_copies(i, stage - 1, True):
                    copy.wait_recv()
            if 0 <= stage <= 3:
                for copy in gather_copies(i, stage, False):
                    copy.start()

    for load in loads:
        load.wait()
    quarter, wide = ext_ref.shape
    width = res_ref.shape[1]
    group = y_count * 2 * quarter

    @pl.loop(0, z_count * 2)
    def _(b):
        block = rows_all[b // 2, lax.rem(b, 2)].reshape(group, wide)
        rows = block[:, :width]
        gate_pre = jnp.dot(rows, gate_w[...], preferred_element_type=jnp.float32)
        up_pre = jnp.dot(rows, up_w[...], preferred_element_type=jnp.float32)
        hidden[b] = clamped_unit(gate_pre, up_pre).astype(jnp.bfloat16)
        lane = lax.broadcasted_iota(jnp.int32, (group, LANES), 1) % (LANES // 2)
        share = jnp.sum(
            jnp.where(lane == sp_me, block[:, width:].astype(jnp.float32), 0.0),
            axis=-1,
            keepdims=True,
        )
        shares[b] = jnp.broadcast_to(share, (group, LANES))

    def order_of(j):
        return ("x", "y") if j % 2 else ("y", "x")

    def reduce_copies(j, stage):
        axis = "c" if stage == 0 else order_of(j)[stage - 1] if stage < 3 else "z"
        if stage == 0:
            src, dst = parts.at[j, :, :, :, 1 - c], got_core.at[j]
        elif stage == 1 and axis == "y":
            src, dst = parts.at[j, :, :, 1 - y, c], got_first.at[j]
        elif stage == 1:
            src, dst = parts.at[j, :, 1 - x, :, c], got_first.at[j]
        elif stage == 2 and axis == "x":
            src, dst = parts.at[j, :, 1 - x, y, c], got_second.at[j]
        elif stage == 2:
            src, dst = parts.at[j, :, x, 1 - y, c], got_second.at[j]
        else:
            return [
                remote(
                    parts.at[j, lax.rem(z + d, z_count), x, y, c], got_z.at[j, d - 1],
                    reduce_send.at[j, 2 + d], reduce_recv.at[j, 2 + d], z_peer(d),
                )
                for d in range(1, z_count)
            ]
        return [
            remote(
                src, dst, reduce_send.at[j, stage], reduce_recv.at[j, stage], partner[axis]
            )
        ]

    def add(ours, theirs):
        return (ours.astype(jnp.float32) + theirs.astype(jnp.float32)).astype(jnp.bfloat16)

    def absorb(j, stage):
        for copy in reduce_copies(j, stage):
            copy.wait_recv()
        if stage == 3:
            cols = slice(reduce_cuts[j][0], reduce_cuts[j][0] + reduce_cuts[j][1])
            total = parts[j, z, x, y, c].astype(jnp.float32)
            for d in range(1, z_count):
                total = total + got_z[j, d - 1].astype(jnp.float32)
            out_ref[:, cols] = (res_ref[:, cols].astype(jnp.float32) + total).astype(jnp.bfloat16)
            return

        @pl.loop(0, z_count)
        def _(zz):
            if stage == 0:
                for xx in range(2):
                    for yy in range(y_count):
                        parts[j, zz, xx, yy, c] = add(
                            parts[j, zz, xx, yy, c], got_core[j, zz, xx, yy]
                        )
            elif stage == 1 and order_of(j)[0] == "y":
                for xx in range(2):
                    parts[j, zz, xx, y, c] = add(parts[j, zz, xx, y, c], got_first[j, zz, xx])
            elif stage == 1:
                for yy in range(y_count):
                    parts[j, zz, x, yy, c] = add(parts[j, zz, x, yy, c], got_first[j, zz, yy])
            else:
                parts[j, zz, x, y, c] = add(parts[j, zz, x, y, c], got_second[j, zz])

    pieces = len(reduce_cuts)
    for tick in range(pieces // 2 + 4):
        for piece in range(2 * tick, min(2 * tick + 2, pieces)):
            at, size = reduce_cuts[piece]

            @pl.loop(0, z_count * 2)
            def _(b):
                out = jnp.dot(
                    hidden[b], down_w[:, at : at + size], preferred_element_type=jnp.float32
                )
                out = (out * shares[b][:, 0:1]).astype(jnp.bfloat16)
                parts[piece, b // 2, lax.rem(b, 2)] = out.reshape(y_count, 2, quarter, size)

            reduce_copies(piece, 0)[0].start()
        for j in range(pieces):
            stage = tick - j // 2
            if 1 <= stage <= 4:
                absorb(j, stage - 1)
                if stage < 4:
                    for copy in reduce_copies(j, stage):
                        copy.start()

    for i in range(chunks):
        for stage in range(4):
            for copy in gather_copies(i, stage, False):
                copy.wait_send()
    for j in range(pieces):
        for stage in range(4):
            for copy in reduce_copies(j, stage):
                copy.wait_send()


def cuts(total, pieces):
    tiles = total // LANES
    edges = [tiles * i // pieces * LANES for i in range(pieces + 1)]
    return [(edges[i], edges[i + 1] - edges[i]) for i in range(pieces)]


def expert_rows(extended, residual, gate_cols, up_cols, down_rows):
    z_count, y_count = lax.axis_size("sp") // 2, lax.axis_size("tp") // 2
    quarter, wide = extended.shape
    width, units = gate_cols.shape
    gather_cuts, reduce_cuts = cuts(wide, 8), cuts(width, 8)
    pieces, size = len(reduce_cuts), reduce_cuts[0][1]
    group = y_count * 2 * quarter
    vmem = pl.BlockSpec(memory_space=pltpu.VMEM)
    hbm = pl.BlockSpec(memory_space=pl.ANY)
    bf16 = jnp.bfloat16
    return pl.pallas_call(
        functools.partial(expert_kernel, z_count, y_count, gather_cuts, reduce_cuts),
        out_shape=jax.ShapeDtypeStruct((quarter, width), bf16),
        in_specs=[vmem, vmem, hbm, hbm, hbm],
        out_specs=vmem,
        scratch_shapes=[
            pltpu.VMEM((z_count, 2, y_count, 2, quarter, wide), bf16),
            pltpu.VMEM(gate_cols.shape, bf16),
            pltpu.VMEM(up_cols.shape, bf16),
            pltpu.VMEM(down_rows.shape, bf16),
            pltpu.VMEM((z_count * 2, group, units), bf16),
            pltpu.VMEM((z_count * 2, group, LANES), jnp.float32),
            pltpu.VMEM((pieces, z_count, 2, y_count, 2, quarter, size), bf16),
            pltpu.VMEM((pieces, z_count, 2, y_count, quarter, size), bf16),
            pltpu.VMEM((pieces, z_count, 2, quarter, size), bf16),
            pltpu.VMEM((pieces, z_count, quarter, size), bf16),
            pltpu.VMEM((pieces, z_count - 1, quarter, size), bf16),
            pltpu.SemaphoreType.DMA((3,)),
            pltpu.SemaphoreType.DMA,
            pltpu.SemaphoreType.DMA((len(gather_cuts), z_count + 3)),
            pltpu.SemaphoreType.DMA((len(gather_cuts), z_count + 3)),
            pltpu.SemaphoreType.DMA((pieces, z_count + 3)),
            pltpu.SemaphoreType.DMA((pieces, z_count + 3)),
        ],
        compiler_params=pltpu.CompilerParams(
            collective_id=1, has_side_effects=True, vmem_limit_bytes=56 << 20
        ),
        name="expert_rows",
    )(extended, residual, gate_cols, up_cols, down_rows)


def slot_ids(routes, capacity, experts):
    batch_size, rows_each, top_count = routes.shape
    flat_ids = routes.reshape(batch_size, rows_each * top_count)
    onehot = (flat_ids[:, :, None] == jnp.arange(experts, dtype=jnp.int32)[None, None, :]).astype(
        jnp.int32
    )
    earlier = jnp.cumsum(onehot, axis=1) - onehot
    rank_in = jnp.sum(earlier * onehot, axis=2)
    return (flat_ids * capacity + rank_in).reshape(batch_size, rows_each, top_count)


def dispatch_rows(slots, row_data, slot_total):
    chosen = jnp.any(slots[..., None] == jnp.arange(slot_total, dtype=jnp.int32), axis=2).astype(
        jnp.bfloat16
    )
    return jnp.einsum("brs,brd->bsd", chosen, row_data, preferred_element_type=jnp.float32).astype(
        jnp.bfloat16
    )


def on_device(
    residual_in,
    queries,
    key_rows,
    value_rows,
    out_gate,
    decay_logit,
    head_gain,
    w_out,
    ffn_gain,
    routing,
    route_weight,
    w_gate,
    w_up,
    w_down,
):
    tp_count = lax.axis_size("tp")
    experts = lax.axis_size("sp")
    quarter = residual_in.shape[0]
    top_count = routing.shape[1]
    model_width = residual_in.shape[1]
    capacity = 2 * routing.shape[0] * top_count // (tp_count * experts)
    slot_total = experts * capacity
    residual, extended = mix_rows(
        queries, key_rows, value_rows, out_gate, decay_logit, head_gain, w_out,
        ffn_gain, routing, route_weight, residual_in,
    )
    if capacity >= quarter and experts <= LANES // 2 and experts % 2 == 0 and tp_count == 4:
        return expert_rows(extended, residual, w_gate[0], w_up[0], w_down[0])
    normed = extended[:, :model_width]
    gate_cols = w_gate[0]
    up_cols = w_up[0]
    down_rows = w_down[0]
    own_routes = lax.dynamic_slice_in_dim(routing, lax.axis_index("tp") * quarter, quarter, 0)
    own_slots = slot_ids(own_routes[None], capacity, experts)[0]
    outgoing = dispatch_rows(own_slots[None], normed[None], slot_total)[0]
    arrived = lax.all_to_all(
        outgoing.reshape(experts, capacity, model_width),
        "sp",
        split_axis=0,
        concat_axis=0,
        tiled=True,
    )
    portion = lax.all_gather(arrived[None], "tp", axis=0, tiled=True)
    flat_rows = portion.reshape(-1, model_width)
    gate_pre = jnp.dot(flat_rows, gate_cols, preferred_element_type=jnp.float32)
    up_pre = jnp.dot(flat_rows, up_cols, preferred_element_type=jnp.float32)
    hidden_rows = clamped_unit(gate_pre, up_pre).astype(jnp.bfloat16)
    hidden = hidden_rows.reshape(portion.shape[:-1] + (gate_cols.shape[1],))
    portion = hidden
    partial_out = jnp.dot(
        portion.reshape(-1, hidden.shape[-1]), down_rows, preferred_element_type=jnp.float32
    ).astype(jnp.bfloat16)
    partial_out = lax.optimization_barrier(partial_out)
    summed = lax.psum_scatter(
        partial_out.astype(jnp.float32)
        .reshape(portion.shape[:-1] + (model_width,))
        .astype(jnp.bfloat16),
        "tp",
        scatter_dimension=0,
        tiled=True,
    ).astype(jnp.float32)
    returned = lax.all_to_all(
        summed[0].astype(jnp.bfloat16), "sp", split_axis=0, concat_axis=0, tiled=True
    )
    picked = jnp.take(
        returned.reshape(slot_total, model_width), own_slots.reshape(-1), axis=0
    ).reshape(quarter, top_count, model_width)
    routed = jnp.sum(picked.astype(jnp.float32) * route_weight[:, :, None], axis=1)
    return (residual.astype(jnp.float32) + routed).astype(jnp.bfloat16)


def solution(mesh):
    placed = (
        P(("sp", "tp"), None),
        P("sp", "tp"),
        P("sp", "tp"),
        P("sp", "tp"),
        P("sp", "tp"),
        P("sp", "tp"),
        P(),
        P(),
        P(),
        P("sp", None),
        P(("sp", "tp"), None),
        P("sp", None, "tp"),
        P("sp", None, "tp"),
        P("sp", "tp", None),
    )
    return jax.shard_map(
        on_device, mesh=mesh, in_specs=placed, out_specs=P(("sp", "tp"), None), check_vma=False
    )
```

profile of v0, /device:TPU:0, one launch (start us, length us, event | category | flops | bytes accessed | tf_op | source)
XLA Modules:
  0.0 152.4 jit_solution(11291792857288101954)
XLA Ops:
  0.0 0.7 reshape.7.ffn_gain_ref
  0.7 0.8 copy.16.weight_ref
  1.5 0.8 copy.15.routing_ref
  2.3 0.0 copy-start
  2.3 2.2 %copy-done = bf16[1024,2048]{1,0:T(8,128)(2,1)S(1)} copy-done((bf16[1024,2048]{1,0:T(8,128)(2,1)S(1)}, bf16[1024,2048]{1,0:T(8,128)(2,1)}, u32[]{:S(2)}) %copy-start) | copy-done | bytes 4194328
  4.5 0.0 copy-start.3
  4.5 0.9 copy-done.3
  5.4 0.0 copy-start.4
  5.4 0.9 copy-done.4
  6.3 0.0 copy-start.5
  6.3 0.9 copy-done.5
  7.2 0.0 copy-start.6
  7.2 0.9 copy-done.6
  8.1 0.0 copy-start.7
  8.1 0.8 copy-done.7
  9.0 0.0 copy-start.8
  9.0 0.8 copy-done.8
  9.8 0.0 copy-start.9
  9.8 0.7 copy-done.9
  10.5 16.6 %mix_rows.1 = (bf16[64,2048]{1,0:T(8,128)(2,1)S(1)}, bf16[64,2176]{1,0:T(8,128)(2,1)S(1)}) custom-call(bf16[256,128]{1,0:T(8,128)(2,1)S(1)} %copy-done.7, bf16[256,128]{1,0:T(8,128)(2,1)S(1)} %copy-done.8, bf16[256,256]{1,0:T(8,128)(2,1)S(1)} %copy-done.4, bf16[256,256]{1,0:T(8,128)(2,1)S(1)} %copy-done.5, f32[256,128]{1,0:T(8,128)S(1)} %copy-done.6, ...), custom_call_target="tpu_custom_call" | custom-call | tf_op jit(solution)/shard_map/mix_rows/pallas_call | solution.py:228
  27.1 0.0 copy-start.1
  27.1 0.7 copy-done.1
  27.8 0.0 copy-start.2
  27.8 0.7 copy-done.2
  28.5 122.2 %expert_rows.1 = bf16[64,2048]{1,0:T(8,128)(2,1)} custom-call(bf16[64,2176]{1,0:T(8,128)(2,1)} %copy-done.1, bf16[64,2048]{1,0:T(8,128)(2,1)} %copy-done.2, bf16[2048,512]{1,0:T(8,128)(2,1)} %bitcast.5, bf16[2048,512]{1,0:T(8,128)(2,1)} %bitcast.6, bf16[512,2048]{1,0:T(8,128)(2,1)} %bitcast.7), custom_call_target="tpu_custom_call" | custom-call | tf_op jit(solution)/shard_map/expert_rows/pallas_call | solution.py:465
  150.8 1.7 %copy.18 = bf16[64,2048]{1,0:T(8,128)(2,1)} copy(bf16[64,2048]{1,0:T(8,128)(2,1)} %expert_rows.1) | data formatting | bytes 524288
Async XLA Ops:
  2.3 2.2 %copy-start = (bf16[1024,2048]{1,0:T(8,128)(2,1)S(1)}, bf16[1024,2048]{1,0:T(8,128)(2,1)}, u32[]{:S(2)}) copy-start(bf16[1024,2048]{1,0:T(8,128)(2,1)} %w_hbm.1) | copy-start | bytes 12582916
  4.5 0.9 copy-start.3
  5.4 0.9 copy-start.4
  6.3 0.9 copy-start.5
  7.2 0.9 copy-start.6
  8.1 0.8 copy-start.7
  9.0 0.8 copy-start.8
  9.8 0.7 copy-start.9
  27.1 0.7 copy-start.1
  27.8 0.7 copy-start.2
where the time goes:
time: 153 us; the launch traced here: 152 us
  Pallas kernels  139 us (91%)
  local copies, waits for them, and re-layouts  13.5 us (9%)
    pallas_call x1, Pallas kernels, expert_rows(): pl.pallas_call(functools.partial(expert_kernel, z_count, y_count, gather_...  122 us
    pallas_call x1, Pallas kernels, mix_rows(): pl.pallas_call(functools.partial(mix_kernel, sp_count, tp_count), out_sha...  16.6 us
    unnamed x23, local copies, waits for them, and re-layouts  12.8 us

commit v1 on v0

--- a/solution.py
+++ b/solution.py
@@ -255,242 +255,503 @@
     )
 
 
-def expert_kernel(
-    z_count, y_count, gather_cuts, reduce_cuts,
-    ext_ref, res_ref, gate_hbm, up_hbm, down_hbm, out_ref,
-    rows_all, gate_w, up_w, down_w, hidden, shares, parts, got_core, got_first, got_second, got_z,
-    w_sem, own_sem, gather_send, gather_recv, reduce_send, reduce_recv,
+GROUP = 16
+SPREAD = ("zxy", "zyx", "xzy", "yzx")
+GATHER_LAG = (0, 2, 4, 7, 8)
+REDUCE_LAG = (0, 1, 3, 6, 8)
+REDUCE_AT = 13
+
+
+def layer_kernel(
+    sp_count, tp_count, cuts,
+    q_hbm, k_hbm, v_hbm, gate_hbm, decay_hbm, head_gain_hbm, w_out_hbm, ffn_gain_hbm,
+    routing_hbm, weight_hbm, res_in_hbm, up_gate_hbm, up_hbm, down_hbm,
+    out_ref,
+    q_ref, k_ref, v_ref, gate_ref, decay_ref, head_gain_ref, ffn_gain_ref,
+    routing_ref, weight_ref, res_ref,
+    states, attended, opened, mixed, mixed_in, w_vmem,
+    rows_all, share_all, gate_w, up_w, down_w, hidden, parts, got_core, got_one, got_two, got_mid, got_last,
+    in_sem, w_sem, state_send, state_recv, mix_send, mix_recv,
+    share_send, share_recv, gather_send, gather_recv, reduce_send, reduce_recv,
 ):
     sp_me, tp_me = lax.axis_index("sp"), lax.axis_index("tp")
+    z_count = sp_count // 2
     z, x = sp_me // 2, lax.rem(sp_me, 2)
     y, c = tp_me // 2, lax.rem(tp_me, 2)
+    barrier = pltpu.get_barrier_semaphore()
+
+    @pl.loop(1, sp_count)
+    def _(d):
+        pl.semaphore_signal(
+            barrier, inc=1, device_id={"sp": lax.rem(sp_me + d, sp_count)}, device_id_type=MESH
+        )
+
+    @pl.loop(1, tp_count)
+    def _(d):
+        pl.semaphore_signal(
+            barrier, inc=1, device_id={"tp": lax.rem(tp_me + d, tp_count)}, device_id_type=MESH
+        )
+
+    small = [
+        pltpu.make_async_copy(src, dst, in_sem.at[i])
+        for i, (src, dst) in enumerate(
+            (
+                (decay_hbm, decay_ref), (k_hbm, k_ref), (v_hbm, v_ref), (q_hbm, q_ref),
+                (routing_hbm, routing_ref), (weight_hbm, weight_ref), (gate_hbm, gate_ref),
+                (head_gain_hbm, head_gain_ref), (ffn_gain_hbm, ffn_gain_ref), (res_in_hbm, res_ref),
+            )
+        )
+    ]
+    large = [
+        pltpu.make_async_copy(src, dst, w_sem.at[i])
+        for i, (src, dst) in enumerate(
+            ((w_out_hbm, w_vmem), (up_gate_hbm, gate_w), (up_hbm, up_w), (down_hbm, down_w))
+        )
+    ]
+    for load in small + large:
+        load.start()
+
+    def remote(src, dst, send, recv, target):
+        return pltpu.make_async_remote_copy(
+            src_ref=src, dst_ref=dst, send_sem=send, recv_sem=recv,
+            device_id=target, device_id_type=MESH,
+        )
+
     partner = {
         "x": {"sp": z * 2 + 1 - x},
         "y": {"tp": (1 - y) * 2 + c},
         "c": {"tp": y * 2 + 1 - c},
     }
-    barrier = pltpu.get_barrier_semaphore()
 
     def z_peer(d):
         return {"sp": lax.rem(z + d, z_count) * 2 + x}
 
-    for target in [z_peer(d) for d in range(1, z_count)] + list(partner.values()):
-        pl.semaphore_signal(barrier, inc=1, device_id=target, device_id_type=MESH)
-    loads = [
-        pltpu.make_async_copy(src, dst, w_sem.at[i])
-        for i, (src, dst) in enumerate(((gate_hbm, gate_w), (up_hbm, up_w), (down_hbm, down_w)))
-    ]
-    own = pltpu.make_async_copy(ext_ref, rows_all.at[z, x, y, c], own_sem)
-    own.start()
-    for load in loads:
-        load.start()
-    own.wait()
-    pl.semaphore_wait(barrier, z_count + 2)
-
-    def remote(src, dst, send, recv, target):
-        return pltpu.make_async_remote_copy(
-            src_ref=src, dst_ref=dst, send_sem=send, recv_sem=recv,
-            device_id=target, device_id_type=MESH,
-        )
-
-    def gather_copies(i, stage, arriving):
-        cols = pl.ds(gather_cuts[i][0], gather_cuts[i][1])
-        order = ("x", "y") if i % 2 else ("y", "x")
-        if stage == 0:
+    tokens, key_lanes = q_ref.shape
+    value_lanes = v_ref.shape[1]
+    rows, width = res_ref.shape
+    head_count = key_lanes // DK
+    lane_head = lax.broadcasted_iota(jnp.int32, (1, key_lanes), 1) // DK
+    small[0].wait()
+    logit = decay_ref[...]
+    log_decay = (jnp.minimum(logit, 0.0) - jnp.log1p(jnp.exp(-jnp.abs(logit)))) / DECAY_TEMP
+    row_id = lax.broadcasted_iota(jnp.int32, (tokens, tokens), 0)
+    col_id = lax.broadcasted_iota(jnp.int32, (tokens, tokens), 1)
+    lower = (row_id >= col_id).astype(jnp.float32)
+    cumulative = jnp.dot(
+        lower, log_decay, precision=EXACT_PRECISION, preferred_element_type=jnp.float32
+    )
+    for load in small[1:]:
+        load.wait()
+    keys = k_ref[...].astype(jnp.float32)
+    query = q_ref[...].astype(jnp.float32) * DK ** (-0.5)
+    values = v_ref[...]
+    ending = cumulative[tokens - 1 :, :]
+    wide = tn_dot(values, (keys * jnp.exp(ending - cumulative)).astype(jnp.bfloat16))
+    state = jnp.zeros((DV, key_lanes), jnp.float32)
+    for h in range(head_count):
+        state = jnp.where(lane_head == h, wide[h * DV : (h + 1) * DV, :], state)
+    passing = jnp.exp(ending)
+    passing_hi = passing.astype(jnp.bfloat16).astype(jnp.float32)
+    tail_row = lax.broadcasted_iota(jnp.int32, (16, key_lanes), 0)
+    tail = jnp.where(
+        tail_row == 0, passing_hi, jnp.where(tail_row == 1, passing - passing_hi, 0.0)
+    )
+    states[sp_me, 0:DV, :] = state.astype(jnp.bfloat16)
+    states[sp_me, DV : DV + 16, :] = tail.astype(jnp.bfloat16)
+
+    pl.semaphore_wait(barrier, sp_count + tp_count - 2)
+
+    def state_copy(slot, d):
+        return remote(
+            states.at[slot], states.at[slot], state_send.at[d], state_recv.at[slot],
+            {"sp": sp_me + d},
+        )
+
+    @pl.loop(1, sp_count - sp_me)
+    def _(d):
+        state_copy(sp_me, d).start()
+
+    lane = lax.broadcasted_iota(jnp.int32, (LANES, tokens), 0)
+    share = jnp.zeros((LANES, tokens), jnp.float32)
+    spot = lax.broadcasted_iota(jnp.int32, (rows, tokens), 1)
+    mine = spot == lax.broadcasted_iota(jnp.int32, (rows, tokens), 0) + tp_me * rows
+    for j in range(weight_ref.shape[0]):
+        weight = jnp.concatenate([weight_ref[j : j + 1, :]] * tp_count, axis=1)
+        share = share + jnp.where(lane % (LANES // 2) == routing_ref[j : j + 1, :], weight, 0.0)
+    share_hi = share.astype(jnp.bfloat16).astype(jnp.float32)
+    share = jnp.where(lane < LANES // 2, share_hi, share - share_hi).astype(jnp.bfloat16)
+    share_all[z, x, y, c] = nt_dot(mine.astype(jnp.bfloat16), share).astype(jnp.bfloat16)
+
+    def spread(ref, lead, cols, order, stage, arriving, send, recv):
+        at = {"z": z, "x": x, "y": y, "c": c}
+        for axis in order[:stage]:
+            at[axis] = slice(None)
+        axis = order[stage]
+
+        def block(place):
+            return ref.at[(*lead, place["z"], place["x"], place["y"], place["c"], slice(None), cols)]
+
+        copies = []
+        if axis == "z":
+            for d in range(1, z_count):
+                src = block({**at, "z": lax.rem(z + z_count - d, z_count)} if arriving else at)
+                copies.append(remote(src, src, send(d - 1), recv(d - 1), z_peer(d)))
+            return copies
+        slot = z_count - 1 + "xyc".index(axis)
+        src = block({**at, axis: 1 - at[axis]} if arriving else at)
+        return [remote(src, src, send(slot), recv(slot), partner[axis])]
+
+    def share_copies(stage, arriving):
+        return spread(
+            share_all, (), slice(None), "zxyc", stage, arriving,
+            lambda i: share_send.at[i], lambda i: share_recv.at[i],
+        )
+
+    def share_step(stage):
+        if stage:
+            for copy in share_copies(stage - 1, True):
+                copy.wait_recv()
+        if stage < 4:
+            for copy in share_copies(stage, False):
+                copy.start()
+
+    share_step(0)
+
+    for i in range(tokens // SUB):
+        first = i * SUB
+        reach = min(-(-(first + SUB) // LANES) * LANES, tokens)
+        start = cumulative[first - 1 : first, :] if i else jnp.zeros((1, key_lanes), jnp.float32)
+        q_sub = query[first : first + SUB] * jnp.exp(cumulative[first : first + SUB] - start)
+        k_sub = keys[:reach] * jnp.exp(jnp.minimum(start - cumulative[:reach], EXP_CAP))
+        stacked = jnp.concatenate(
+            [jnp.where(lane_head == h, q_sub, 0.0) for h in range(head_count)], axis=0
+        )
+        scores = nt_dot(stacked.astype(jnp.bfloat16), k_sub.astype(jnp.bfloat16))
+        at_row = lax.broadcasted_iota(jnp.int32, scores.shape, 0) % SUB + first
+        at_col = lax.broadcasted_iota(jnp.int32, scores.shape, 1)
+        scores = jnp.where(at_row >= at_col, scores, 0.0).astype(jnp.bfloat16)
+        inner = jnp.dot(scores, values[:reach], preferred_element_type=jnp.float32)
+        for h in range(head_count):
+            attended[first : first + SUB, h * DV : (h + 1) * DV] = inner[
+                h * SUB : (h + 1) * SUB, h * DV : (h + 1) * DV
+            ]
+    for h in range(head_count):
+        cols = slice(h * DV, (h + 1) * DV)
+        wide_gate = gate_ref[:, cols].astype(jnp.float32)
+        opened[:, cols] = (
+            head_gain_ref[...].astype(jnp.float32) * wide_gate * jax.nn.sigmoid(wide_gate)
+        )
+    share_step(1)
+
+    @pl.loop(0, sp_me)
+    def _(j):
+        state_copy(j, 0).wait_recv()
+
+    def absorb(j, incoming):
+        decay = states[j, DV : DV + 16, :].astype(jnp.float32)
+        total = decay[0:1, :] + decay[1:2, :]
+        return total * incoming + states[j, 0:DV, :].astype(jnp.float32)
+
+    incoming = lax.fori_loop(
+        0, sp_me, absorb, jnp.zeros((DV, key_lanes), jnp.float32)
+    ).astype(jnp.bfloat16)
+    query_dec = query * jnp.exp(cumulative)
+    for h in range(head_count):
+        cols = slice(h * DV, (h + 1) * DV)
+        readout = nt_dot(jnp.where(lane_head == h, query_dec, 0.0).astype(jnp.bfloat16), incoming)
+        head = attended[:, cols] + readout
+        scale = lax.rsqrt(jnp.mean(head * head, axis=-1, keepdims=True) + NORM_EPS)
+        mixed[:, cols] = (head * scale * opened[:, cols]).astype(jnp.bfloat16)
+
+    def mix_copy(block, slot, d):
+        return remote(
+            mixed.at[pl.ds(pl.multiple_of(block * rows, rows), rows)], mixed_in.at[slot],
+            mix_send.at[d], mix_recv.at[slot], {"tp": lax.rem(tp_me + d, tp_count)},
+        )
+
+    for d in range(1, tp_count):
+        mix_copy(lax.rem(tp_me + d, tp_count), tp_me, d).start()
+    share_step(2)
+    large[0].wait()
+
+    def w_rows(j):
+        return w_vmem[pl.ds(pl.multiple_of(j * value_lanes, value_lanes), value_lanes), :]
+
+    projected = jnp.dot(
+        mixed[pl.ds(pl.multiple_of(tp_me * rows, rows), rows), :],
+        w_rows(tp_me),
+        preferred_element_type=jnp.float32,
+    )
+    for d in range(1, tp_count):
+        slot = lax.rem(tp_me + d, tp_count)
+        mix_copy(slot, slot, d).wait_recv()
+        projected = projected + jnp.dot(
+            mixed_in[slot], w_rows(slot), preferred_element_type=jnp.float32
+        )
+    residual = (res_ref[...].astype(jnp.float32) + projected).astype(jnp.bfloat16)
+    res_ref[...] = residual
+    wide_res = residual.astype(jnp.float32)
+    inv = lax.rsqrt(jnp.mean(wide_res * wide_res, axis=-1, keepdims=True) + NORM_EPS)
+    groups = rows // GROUP
+    for k in range(width // LANES):
+        cols = slice(k * LANES, (k + 1) * LANES)
+        normed = wide_res[:, cols] * inv * ffn_gain_ref[k : k + 1, :].astype(jnp.float32)
+        normed = normed.astype(jnp.bfloat16)
+        for g in range(groups):
+            rows_all[g, z, x, y, c, :, cols] = normed[g * GROUP : (g + 1) * GROUP]
+
+    chunks = len(SPREAD)
+
+    def span(q):
+        return pl.ds(cuts[q][0], cuts[q][1])
+
+    def gather_copies(g, q, stage, arriving):
+        return spread(
+            rows_all, (g,), span(q), SPREAD[q] + "c", stage, arriving,
+            lambda i: gather_send.at[g, q, i], lambda i: gather_recv.at[g, q, i],
+        )
+
+    def gather_step(g, q, stage):
+        if stage:
+            for copy in gather_copies(g, q, stage - 1, True):
+                copy.wait_recv()
+        if stage < 4:
+            for copy in gather_copies(g, q, stage, False):
+                copy.start()
+
+    group_rows = sp_count * tp_count * GROUP
+    half_rows = group_rows // 2
+    half_z = z_count // 2
+
+    def raise_half(g, half):
+        zs = slice(half * half_z, (half + 1) * half_z)
+        block = rows_all[g, zs].reshape(half_rows, width)
+        gate_pre = jnp.dot(block, gate_w[...], preferred_element_type=jnp.float32)
+        up_pre = jnp.dot(block, up_w[...], preferred_element_type=jnp.float32)
+        tags = share_all[zs, :, :, :, pl.ds(pl.multiple_of(g * GROUP, GROUP), GROUP), :]
+        tags = tags.reshape(half_rows, LANES).astype(jnp.float32)
+        lane = lax.broadcasted_iota(jnp.int32, (half_rows, LANES), 1) % (LANES // 2)
+        share = jnp.sum(jnp.where(lane == sp_me, tags, 0.0), axis=-1, keepdims=True)
+        hidden[g, half * half_rows : (half + 1) * half_rows] = (
+            clamped_unit(gate_pre, up_pre) * share
+        ).astype(jnp.bfloat16)
+
+    def lower_chunk(g, q):
+        at, size = cuts[q]
+        out = jnp.dot(hidden[g], down_w[:, at : at + size], preferred_element_type=jnp.float32)
+        parts[g, :, :, :, :, :, at : at + size] = out.astype(jnp.bfloat16).reshape(
+            z_count, 2, 2, 2, GROUP, size
+        )
+
+    every = slice(None)
+
+    def reduce_order(q):
+        return "c" + SPREAD[q][::-1]
+
+    def reduce_copies(g, q, stage):
+        order, cols = reduce_order(q), span(q)
+        at = {"z": every, "x": every, "y": every, "c": every}
+        for axis in order[:stage]:
+            at[axis] = {"z": z, "x": x, "y": y, "c": c}[axis]
+        axis = order[stage]
+
+        def block(place):
+            return parts.at[g, place["z"], place["x"], place["y"], place["c"], :, cols]
+
+        if axis == "z":
             copies = []
             for d in range(1, z_count):
-                zz = lax.rem(z + z_count - d, z_count) if arriving else z
-                block = rows_all.at[zz, x, y, c, :, cols]
+                dst = got_mid.at[g, d - 1, :, :, cols] if stage == 2 else got_last.at[g, d - 1, :, cols]
                 copies.append(
-                    remote(block, block, gather_send.at[i, d], gather_recv.at[i, d], z_peer(d))
+                    remote(
+                        block({**at, "z": lax.rem(z + d, z_count)}), dst,
+                        reduce_send.at[g, q, d - 1], reduce_recv.at[g, q, d - 1], z_peer(d),
+                    )
                 )
             return copies
-        axis = order[stage - 1] if stage < 3 else "c"
-        xx = 1 - x if arriving and axis == "x" else x
-        yy = 1 - y if arriving and axis == "y" else y
-        cc = 1 - c if arriving and axis == "c" else c
-        if stage == 1:
-            block = rows_all.at[:, xx, yy, cc, :, cols]
-        elif stage == 2 and axis == "x":
-            block = rows_all.at[:, xx, :, cc, :, cols]
-        elif stage == 2:
-            block = rows_all.at[:, :, yy, cc, :, cols]
-        else:
-            block = rows_all.at[:, :, :, cc, :, cols]
-        sem = z_count - 1 + stage
-        return [
-            remote(block, block, gather_send.at[i, sem], gather_recv.at[i, sem], partner[axis])
-        ]
-
-    chunks = len(gather_cuts)
-    for tick in range(chunks // 2 + 4):
-        for i in range(chunks):
-            stage = tick - i // 2
-            if 1 <= stage <= 4:
-                for copy in gather_copies(i, stage - 1, True):
-                    copy.wait_recv()
-            if 0 <= stage <= 3:
-                for copy in gather_copies(i, stage, False):
-                    copy.start()
-
-    for load in loads:
-        load.wait()
-    quarter, wide = ext_ref.shape
-    width = res_ref.shape[1]
-    group = y_count * 2 * quarter
-
-    @pl.loop(0, z_count * 2)
-    def _(b):
-        block = rows_all[b // 2, lax.rem(b, 2)].reshape(group, wide)
-        rows = block[:, :width]
-        gate_pre = jnp.dot(rows, gate_w[...], preferred_element_type=jnp.float32)
-        up_pre = jnp.dot(rows, up_w[...], preferred_element_type=jnp.float32)
-        hidden[b] = clamped_unit(gate_pre, up_pre).astype(jnp.bfloat16)
-        lane = lax.broadcasted_iota(jnp.int32, (group, LANES), 1) % (LANES // 2)
-        share = jnp.sum(
-            jnp.where(lane == sp_me, block[:, width:].astype(jnp.float32), 0.0),
-            axis=-1,
-            keepdims=True,
-        )
-        shares[b] = jnp.broadcast_to(share, (group, LANES))
-
-    def order_of(j):
-        return ("x", "y") if j % 2 else ("y", "x")
-
-    def reduce_copies(j, stage):
-        axis = "c" if stage == 0 else order_of(j)[stage - 1] if stage < 3 else "z"
-        if stage == 0:
-            src, dst = parts.at[j, :, :, :, 1 - c], got_core.at[j]
-        elif stage == 1 and axis == "y":
-            src, dst = parts.at[j, :, :, 1 - y, c], got_first.at[j]
-        elif stage == 1:
-            src, dst = parts.at[j, :, 1 - x, :, c], got_first.at[j]
-        elif stage == 2 and axis == "x":
-            src, dst = parts.at[j, :, 1 - x, y, c], got_second.at[j]
-        elif stage == 2:
-            src, dst = parts.at[j, :, x, 1 - y, c], got_second.at[j]
-        else:
-            return [
-                remote(
-                    parts.at[j, lax.rem(z + d, z_count), x, y, c], got_z.at[j, d - 1],
-                    reduce_send.at[j, 2 + d], reduce_recv.at[j, 2 + d], z_peer(d),
-                )
-                for d in range(1, z_count)
-            ]
+        own = {"x": x, "y": y, "c": c}[axis]
+        dst = (
+            got_core.at[g, :, :, :, :, cols] if stage == 0
+            else got_one.at[g, :, :, :, cols] if stage == 1
+            else got_two.at[g, :, :, cols] if stage == 2
+            else got_last.at[g, 0, :, cols]
+        )
+        slot = z_count - 1 + "xyc".index(axis)
         return [
             remote(
-                src, dst, reduce_send.at[j, stage], reduce_recv.at[j, stage], partner[axis]
+                block({**at, axis: 1 - own}), dst,
+                reduce_send.at[g, q, slot], reduce_recv.at[g, q, slot], partner[axis],
             )
         ]
 
-    def add(ours, theirs):
-        return (ours.astype(jnp.float32) + theirs.astype(jnp.float32)).astype(jnp.bfloat16)
-
-    def absorb(j, stage):
-        for copy in reduce_copies(j, stage):
+    def f32(value):
+        return value.astype(jnp.float32)
+
+    def absorb_step(g, q, stage):
+        for copy in reduce_copies(g, q, stage):
             copy.wait_recv()
-        if stage == 3:
-            cols = slice(reduce_cuts[j][0], reduce_cuts[j][0] + reduce_cuts[j][1])
-            total = parts[j, z, x, y, c].astype(jnp.float32)
+        order = reduce_order(q)
+        at, size = cuts[q]
+        cols = slice(at, at + size)
+        if stage == 0:
+            @pl.loop(0, z_count)
+            def _(zz):
+                ours = parts[g, zz, :, :, c, :, cols]
+                parts[g, zz, :, :, c, :, cols] = (
+                    f32(ours) + f32(got_core[g, zz, :, :, :, cols])
+                ).astype(jnp.bfloat16)
+        elif stage == 1:
+            where = (g, every, x, every, c) if order[1] == "x" else (g, every, every, y, c)
+            where = (*where, every, cols)
+            parts[where] = (f32(parts[where]) + f32(got_one[g, :, :, :, cols])).astype(jnp.bfloat16)
+        elif stage == 2 and order[2] != "z":
+            where = (g, every, x, y, c, every, cols)
+            parts[where] = (f32(parts[where]) + f32(got_two[g, :, :, cols])).astype(jnp.bfloat16)
+        elif stage == 2:
+            where = (g, z, x, every, c) if order[1] == "x" else (g, z, every, y, c)
+            where = (*where, every, cols)
+            total = f32(parts[where])
             for d in range(1, z_count):
-                total = total + got_z[j, d - 1].astype(jnp.float32)
-            out_ref[:, cols] = (res_ref[:, cols].astype(jnp.float32) + total).astype(jnp.bfloat16)
-            return
-
-        @pl.loop(0, z_count)
-        def _(zz):
-            if stage == 0:
-                for xx in range(2):
-                    for yy in range(y_count):
-                        parts[j, zz, xx, yy, c] = add(
-                            parts[j, zz, xx, yy, c], got_core[j, zz, xx, yy]
-                        )
-            elif stage == 1 and order_of(j)[0] == "y":
-                for xx in range(2):
-                    parts[j, zz, xx, y, c] = add(parts[j, zz, xx, y, c], got_first[j, zz, xx])
-            elif stage == 1:
-                for yy in range(y_count):
-                    parts[j, zz, x, yy, c] = add(parts[j, zz, x, yy, c], got_first[j, zz, yy])
-            else:
-                parts[j, zz, x, y, c] = add(parts[j, zz, x, y, c], got_second[j, zz])
-
-    pieces = len(reduce_cuts)
-    for tick in range(pieces // 2 + 4):
-        for piece in range(2 * tick, min(2 * tick + 2, pieces)):
-            at, size = reduce_cuts[piece]
-
-            @pl.loop(0, z_count * 2)
-            def _(b):
-                out = jnp.dot(
-                    hidden[b], down_w[:, at : at + size], preferred_element_type=jnp.float32
-                )
-                out = (out * shares[b][:, 0:1]).astype(jnp.bfloat16)
-                parts[piece, b // 2, lax.rem(b, 2)] = out.reshape(y_count, 2, quarter, size)
-
-            reduce_copies(piece, 0)[0].start()
-        for j in range(pieces):
-            stage = tick - j // 2
-            if 1 <= stage <= 4:
-                absorb(j, stage - 1)
-                if stage < 4:
-                    for copy in reduce_copies(j, stage):
-                        copy.start()
-
-    for i in range(chunks):
-        for stage in range(4):
-            for copy in gather_copies(i, stage, False):
-                copy.wait_send()
-    for j in range(pieces):
-        for stage in range(4):
-            for copy in reduce_copies(j, stage):
-                copy.wait_send()
-
-
-def cuts(total, pieces):
-    tiles = total // LANES
-    edges = [tiles * i // pieces * LANES for i in range(pieces + 1)]
-    return [(edges[i], edges[i + 1] - edges[i]) for i in range(pieces)]
-
-
-def expert_rows(extended, residual, gate_cols, up_cols, down_rows):
-    z_count, y_count = lax.axis_size("sp") // 2, lax.axis_size("tp") // 2
-    quarter, wide = extended.shape
-    width, units = gate_cols.shape
-    gather_cuts, reduce_cuts = cuts(wide, 8), cuts(width, 8)
-    pieces, size = len(reduce_cuts), reduce_cuts[0][1]
-    group = y_count * 2 * quarter
+                total = total + f32(got_mid[g, d - 1, :, :, cols])
+            parts[where] = total.astype(jnp.bfloat16)
+        else:
+            total = f32(parts[g, z, x, y, c, :, cols])
+            for d in range(1, z_count if order[3] == "z" else 2):
+                total = total + f32(got_last[g, d - 1, :, cols])
+            here = pl.ds(pl.multiple_of(g * GROUP, GROUP), GROUP)
+            out_ref[here, cols] = (f32(res_ref[here, cols]) + total).astype(jnp.bfloat16)
+
+    def reduce_step(g, q, stage):
+        if stage:
+            absorb_step(g, q, stage - 1)
+        if stage < 4:
+            for copy in reduce_copies(g, q, stage):
+                copy.start()
+
+    def at_lag(it, q, lag, step):
+        g = it + (q - lag) // chunks
+
+        @pl.when((g >= 0) & (g < groups))
+        def _():
+            step(g, (q - lag) % chunks)
+
+    last = groups * chunks - 1 + REDUCE_AT + REDUCE_LAG[4]
+    share_step(3)
+
+    @pl.loop(0, last // chunks + 1)
+    def _(it):
+        @pl.when(it == 2)
+        def _():
+            share_step(4)
+            for load in large[1:]:
+                load.wait()
+
+        for q in range(chunks):
+            for stage in (0, 1, 2, 3, 4):
+                at_lag(it, q, GATHER_LAG[stage], functools.partial(gather_step, stage=stage))
+            if q == chunks - 1:
+                at_lag(it, q, GATHER_LAG[4], lambda g, _: raise_half(g, 0))
+            if q == 0:
+                at_lag(it, q, GATHER_LAG[4] + 1, lambda g, _: raise_half(g, 1))
+            at_lag(it, q, REDUCE_AT, lower_chunk)
+            for stage in (0, 1, 2, 3, 4):
+                at_lag(it, q, REDUCE_AT + REDUCE_LAG[stage], functools.partial(reduce_step, stage=stage))
+
+    @pl.loop(1, sp_count - sp_me)
+    def _(d):
+        state_copy(sp_me, d).wait_send()
+
+    for d in range(1, tp_count):
+        mix_copy(lax.rem(tp_me + d, tp_count), tp_me, d).wait_send()
+    for stage in range(4):
+        for copy in share_copies(stage, False):
+            copy.wait_send()
+
+    @pl.loop(0, groups)
+    def _(g):
+        for q in range(chunks):
+            for stage in range(4):
+                for copy in gather_copies(g, q, stage, False):
+                    copy.wait_send()
+                for copy in reduce_copies(g, q, stage):
+                    copy.wait_send()
+
+
+def column_cuts(width):
+    tiles = width // LANES
+    edges = [tiles * share // 16 * LANES for share in (0, 5, 10, 13, 16)]
+    return [(edges[i], edges[i + 1] - edges[i]) for i in range(4)]
+
+
+def layer_rows(
+    queries, key_rows, value_rows, out_gate, decay_logit, head_gain, w_out,
+    ffn_gain, routing, route_weight, residual_in, gate_cols, up_cols, down_rows,
+):
+    sp_count, tp_count = lax.axis_size("sp"), lax.axis_size("tp")
+    rows, width = residual_in.shape
+    tokens, key_lanes = queries.shape
+    value_lanes = value_rows.shape[1]
+    units = gate_cols.shape[1]
+    z_count, groups = sp_count // 2, rows // GROUP
+    group_rows = sp_count * tp_count * GROUP
+    cuts = column_cuts(width)
+    hbm = pl.BlockSpec(memory_space=pl.ANY)
     vmem = pl.BlockSpec(memory_space=pltpu.VMEM)
-    hbm = pl.BlockSpec(memory_space=pl.ANY)
-    bf16 = jnp.bfloat16
+    bf16, f32 = jnp.bfloat16, jnp.float32
+    dma = pltpu.SemaphoreType.DMA
+    ways = z_count + 2
+    operands = (
+        queries, key_rows, value_rows, out_gate, decay_logit, head_gain.reshape(1, -1), w_out,
+        ffn_gain.reshape(-1, LANES), routing.T, route_weight.T, residual_in,
+        gate_cols, up_cols, down_rows,
+    )
+
+    def like(array):
+        return pltpu.VMEM(array.shape, array.dtype)
+
     return pl.pallas_call(
-        functools.partial(expert_kernel, z_count, y_count, gather_cuts, reduce_cuts),
-        out_shape=jax.ShapeDtypeStruct((quarter, width), bf16),
-        in_specs=[vmem, vmem, hbm, hbm, hbm],
+        functools.partial(layer_kernel, sp_count, tp_count, cuts),
+        out_shape=jax.ShapeDtypeStruct((rows, width), bf16),
+        in_specs=[hbm] * len(operands),
         out_specs=vmem,
         scratch_shapes=[
-            pltpu.VMEM((z_count, 2, y_count, 2, quarter, wide), bf16),
-            pltpu.VMEM(gate_cols.shape, bf16),
-            pltpu.VMEM(up_cols.shape, bf16),
-            pltpu.VMEM(down_rows.shape, bf16),
-            pltpu.VMEM((z_count * 2, group, units), bf16),
-            pltpu.VMEM((z_count * 2, group, LANES), jnp.float32),
-            pltpu.VMEM((pieces, z_count, 2, y_count, 2, quarter, size), bf16),
-            pltpu.VMEM((pieces, z_count, 2, y_count, quarter, size), bf16),
-            pltpu.VMEM((pieces, z_count, 2, quarter, size), bf16),
-            pltpu.VMEM((pieces, z_count, quarter, size), bf16),
-            pltpu.VMEM((pieces, z_count - 1, quarter, size), bf16),
-            pltpu.SemaphoreType.DMA((3,)),
-            pltpu.SemaphoreType.DMA,
-            pltpu.SemaphoreType.DMA((len(gather_cuts), z_count + 3)),
-            pltpu.SemaphoreType.DMA((len(gather_cuts), z_count + 3)),
-            pltpu.SemaphoreType.DMA((pieces, z_count + 3)),
-            pltpu.SemaphoreType.DMA((pieces, z_count + 3)),
+            *(like(operands[i]) for i in (0, 1, 2, 3, 4, 5, 7, 8, 9, 10)),
+            pltpu.VMEM((sp_count, DV + 16, key_lanes), bf16),
+            pltpu.VMEM((tokens, value_lanes), f32),
+            pltpu.VMEM((tokens, value_lanes), f32),
+            pltpu.VMEM((tokens, value_lanes), bf16),
+            pltpu.VMEM((tp_count, rows, value_lanes), bf16),
+            like(w_out),
+            pltpu.VMEM((groups, z_count, 2, 2, 2, GROUP, width), bf16),
+            pltpu.VMEM((z_count, 2, 2, 2, rows, LANES), bf16),
+            like(gate_cols),
+            like(up_cols),
+            like(down_rows),
+            pltpu.VMEM((groups, group_rows, units), bf16),
+            pltpu.VMEM((groups, z_count, 2, 2, 2, GROUP, width), bf16),
+            pltpu.VMEM((groups, z_count, 2, 2, GROUP, width), bf16),
+            pltpu.VMEM((groups, z_count, 2, GROUP, width), bf16),
+            pltpu.VMEM((groups, z_count, GROUP, width), bf16),
+            pltpu.VMEM((groups, z_count - 1, 2, GROUP, width), bf16),
+            pltpu.VMEM((groups, z_count - 1, GROUP, width), bf16),
+            dma((10,)),
+            dma((4,)),
+            dma((sp_count,)),
+            dma((sp_count,)),
+            dma((tp_count,)),
+            dma((tp_count,)),
+            dma((ways,)),
+            dma((ways,)),
+            dma((groups, 4, ways)),
+            dma((groups, 4, ways)),
+            dma((groups, 4, ways)),
+            dma((groups, 4, ways)),
         ],
         compiler_params=pltpu.CompilerParams(
-            collective_id=1, has_side_effects=True, vmem_limit_bytes=56 << 20
+            collective_id=1, has_side_effects=True, vmem_limit_bytes=62 << 20
         ),
-        name="expert_rows",
-    )(extended, residual, gate_cols, up_cols, down_rows)
+        name="layer_rows",
+    )(*operands)
 
 
 def slot_ids(routes, capacity, experts):
@@ -536,12 +797,18 @@
     model_width = residual_in.shape[1]
     capacity = 2 * routing.shape[0] * top_count // (tp_count * experts)
     slot_total = experts * capacity
+    if (
+        capacity >= quarter and experts <= LANES // 2 and experts % 4 == 0
+        and tp_count == 4 and quarter % GROUP == 0
+    ):
+        return layer_rows(
+            queries, key_rows, value_rows, out_gate, decay_logit, head_gain, w_out,
+            ffn_gain, routing, route_weight, residual_in, w_gate[0], w_up[0], w_down[0],
+        )
     residual, extended = mix_rows(
         queries, key_rows, value_rows, out_gate, decay_logit, head_gain, w_out,
         ffn_gain, routing, route_weight, residual_in,
     )
-    if capacity >= quarter and experts <= LANES // 2 and experts % 2 == 0 and tp_count == 4:
-        return expert_rows(extended, residual, w_gate[0], w_up[0], w_down[0])
     normed = extended[:, :model_width]
     gate_cols = w_gate[0]
     up_cols = w_up[0]

time: 153 us -> 117 us (0.76)
  Pallas kernels: 139 us -> 115 us
  local copies, waits for them, and re-layouts: 13.5 us -> 1.67 us
    pallas_call x2 -> x1, Pallas kernels: 139 us -> 115 us  [layer_rows(): pl.pallas_call(functools.partial(layer_kernel, sp_count, tp_count, cuts),...]
    unnamed x23 -> x1, local copies, waits for them, and re-layouts: 12.8 us -> 1.67 us
where the time goes in v1:
time: 117 us; the launch traced here: 116 us
  Pallas kernels  115 us (98%)
  local copies, waits for them, and re-layouts  1.67 us (1%)
    pallas_call x1, Pallas kernels, layer_rows(): pl.pallas_call(functools.partial(layer_kernel, sp_count, tp_count, cuts),...  115 us

profile of v1, /device:TPU:0, one launch (start us, length us, event | category | flops | bytes accessed | tf_op | source)
XLA Modules:
  0.0 116.4 jit_solution(7353386803894062692)
XLA Ops:
  0.0 114.7 %layer_rows.1 = bf16[64,2048]{1,0:T(8,128)(2,1)} custom-call(bf16[256,128]{1,0:T(8,128)(2,1)} %q_hbm.1, bf16[256,128]{1,0:T(8,128)(2,1)} %k_hbm.1, bf16[256,256]{1,0:T(8,128)(2,1)} %v_hbm.1, bf16[256,256]{1,0:T(8,128)(2,1)} %gate_hbm.1, f32[256,128]{1,0:T(8,128)} %decay_hbm.1, bf16[1,128]{1,0:T(2,128)(2,1)} %bitcast.13, bf16[1024,2048]{1,0:T(8,128)(2,1)} %w_out_hbm.1, ...), custom_call_target="tpu_custom_call" | custom-call | tf_op jit(solution)/shard_map/layer_rows/pallas_call | solution.py:712
  114.7 1.7 %copy.16 = bf16[64,2048]{1,0:T(8,128)(2,1)} copy(bf16[64,2048]{1,0:T(8,128)(2,1)} %layer_rows.1) | data formatting | bytes 524288

commit v2 on v1

--- a/solution.py
+++ b/solution.py
@@ -256,10 +256,13 @@
 
 
 GROUP = 16
-SPREAD = ("zxy", "zyx", "xzy", "yzx")
-GATHER_LAG = (0, 2, 4, 7, 8)
-REDUCE_LAG = (0, 1, 3, 6, 8)
-REDUCE_AT = 13
+PIECES = (('zxy', 5), ('zyx', 5), ('xzy', 3), ('yzx', 3))
+SPREAD = tuple(order for order, _ in PIECES)
+GATHER_PACE, REDUCE_PACE, RAISE_GAP = 5.93, 0.99, 0.74
+GATHER_AT = ((-0.39, 3.6, 7.61, 22.71, 27.52), (-0.09, 7.59, 11.49, 18.04, 27.81), (-10.56, 9.95, 16.61, 26.65, 28.74), (-4.53, 8.4, 15.26, 20.77, 24.71))
+REDUCE_AT = ((0.0, 1.36, 6.01, 10.78, 26.83), (0.43, 4.07, 10.15, 15.03, 38.01), (0.86, 3.15, 8.38, 17.57, 24.05), (1.29, 3.51, 6.46, 16.56, 22.03))
+REDUCE_FROM = 7.8
+SHARE_AT = (-1.71, 2.61, 4.03, 15.57, 17.98)
 
 
 def layer_kernel(
@@ -270,9 +273,9 @@
     q_ref, k_ref, v_ref, gate_ref, decay_ref, head_gain_ref, ffn_gain_ref,
     routing_ref, weight_ref, res_ref,
     states, attended, opened, mixed, mixed_in, w_vmem,
-    rows_all, share_all, gate_w, up_w, down_w, hidden, parts, got_core, got_one, got_two, got_mid, got_last,
+    rows_all, share_all, gate_w, up_w, down_w, hidden, parts, got_core, got_one, got_two, got_mid, got_last, out_rows,
     in_sem, w_sem, state_send, state_recv, mix_send, mix_recv,
-    share_send, share_recv, gather_send, gather_recv, reduce_send, reduce_recv,
+    share_send, share_recv, gather_send, gather_recv, swap_recv, reduce_send, reduce_recv, out_sem,
 ):
     sp_me, tp_me = lax.axis_index("sp"), lax.axis_index("tp")
     z_count = sp_count // 2
@@ -336,9 +339,18 @@
     log_decay = (jnp.minimum(logit, 0.0) - jnp.log1p(jnp.exp(-jnp.abs(logit)))) / DECAY_TEMP
     row_id = lax.broadcasted_iota(jnp.int32, (tokens, tokens), 0)
     col_id = lax.broadcasted_iota(jnp.int32, (tokens, tokens), 1)
-    lower = (row_id >= col_id).astype(jnp.float32)
-    cumulative = jnp.dot(
-        lower, log_decay, precision=EXACT_PRECISION, preferred_element_type=jnp.float32
+    lower = jnp.where(row_id >= col_id, 1.0, 0.0).astype(jnp.bfloat16)
+    top = log_decay.astype(jnp.bfloat16)
+    rest = log_decay - top.astype(jnp.float32)
+    middle = rest.astype(jnp.bfloat16)
+    bottom = (rest - middle.astype(jnp.float32)).astype(jnp.bfloat16)
+    sums = jnp.dot(
+        lower,
+        jnp.concatenate([top, middle, bottom], axis=1),
+        preferred_element_type=jnp.float32,
+    )
+    cumulative = (
+        sums[:, 2 * key_lanes :] + sums[:, key_lanes : 2 * key_lanes] + sums[:, :key_lanes]
     )
     for load in small[1:]:
         load.wait()
@@ -363,11 +375,11 @@
 
     def state_copy(slot, d):
         return remote(
-            states.at[slot], states.at[slot], state_send.at[d], state_recv.at[slot],
-            {"sp": sp_me + d},
-        )
-
-    @pl.loop(1, sp_count - sp_me)
+            states.at[slot], states.at[slot], state_send, state_recv,
+            {"sp": lax.rem(sp_me + d, sp_count)},
+        )
+
+    @pl.loop(1, sp_count)
     def _(d):
         state_copy(sp_me, d).start()
 
@@ -391,20 +403,19 @@
         def block(place):
             return ref.at[(*lead, place["z"], place["x"], place["y"], place["c"], slice(None), cols)]
 
-        copies = []
+        if axis == "z" and arriving:
+            src = block({**at, "z": slice(0, z_count - 1)})
+            return [remote(src, src, send, recv, partner["x"])]
+        src = block(at)
         if axis == "z":
-            for d in range(1, z_count):
-                src = block({**at, "z": lax.rem(z + z_count - d, z_count)} if arriving else at)
-                copies.append(remote(src, src, send(d - 1), recv(d - 1), z_peer(d)))
-            return copies
-        slot = z_count - 1 + "xyc".index(axis)
-        src = block({**at, axis: 1 - at[axis]} if arriving else at)
-        return [remote(src, src, send(slot), recv(slot), partner[axis])]
+            return [remote(src, src, send, recv, z_peer(d)) for d in range(1, z_count)]
+        if arriving:
+            src = block({**at, axis: 1 - at[axis]})
+        return [remote(src, src, send, recv, partner[axis])]
 
     def share_copies(stage, arriving):
         return spread(
-            share_all, (), slice(None), "zxyc", stage, arriving,
-            lambda i: share_send.at[i], lambda i: share_recv.at[i],
+            share_all, (), slice(None), "zxyc", stage, arriving, share_send, share_recv.at[stage],
         )
 
     def share_step(stage):
@@ -415,7 +426,6 @@
             for copy in share_copies(stage, False):
                 copy.start()
 
-    share_step(0)
 
     for i in range(tokens // SUB):
         first = i * SUB
@@ -441,11 +451,9 @@
         opened[:, cols] = (
             head_gain_ref[...].astype(jnp.float32) * wide_gate * jax.nn.sigmoid(wide_gate)
         )
-    share_step(1)
-
-    @pl.loop(0, sp_me)
-    def _(j):
-        state_copy(j, 0).wait_recv()
+    others = states.at[0 : sp_count - 1]
+    state_all = remote(others, others, state_send, state_recv, partner["x"])
+    state_all.wait_recv()
 
     def absorb(j, incoming):
         decay = states[j, DV : DV + 16, :].astype(jnp.float32)
@@ -466,12 +474,11 @@
     def mix_copy(block, slot, d):
         return remote(
             mixed.at[pl.ds(pl.multiple_of(block * rows, rows), rows)], mixed_in.at[slot],
-            mix_send.at[d], mix_recv.at[slot], {"tp": lax.rem(tp_me + d, tp_count)},
+            mix_send, mix_recv, {"tp": lax.rem(tp_me + d, tp_count)},
         )
 
     for d in range(1, tp_count):
-        mix_copy(lax.rem(tp_me + d, tp_count), tp_me, d).start()
-    share_step(2)
+        mix_copy(lax.rem(tp_me + d, tp_count), tp_count - d - 1, d).start()
     large[0].wait()
 
     def w_rows(j):
@@ -482,11 +489,13 @@
         w_rows(tp_me),
         preferred_element_type=jnp.float32,
     )
+    incoming_mix = mixed_in.at[0 : tp_count - 1]
+    mix_all = remote(incoming_mix, incoming_mix, mix_send, mix_recv, partner["c"])
+    mix_all.wait_recv()
     for d in range(1, tp_count):
         slot = lax.rem(tp_me + d, tp_count)
-        mix_copy(slot, slot, d).wait_recv()
         projected = projected + jnp.dot(
-            mixed_in[slot], w_rows(slot), preferred_element_type=jnp.float32
+            mixed_in[d - 1], w_rows(slot), preferred_element_type=jnp.float32
         )
     residual = (res_ref[...].astype(jnp.float32) + projected).astype(jnp.bfloat16)
     res_ref[...] = residual
@@ -508,16 +517,25 @@
     def gather_copies(g, q, stage, arriving):
         return spread(
             rows_all, (g,), span(q), SPREAD[q] + "c", stage, arriving,
-            lambda i: gather_send.at[g, q, i], lambda i: gather_recv.at[g, q, i],
+            gather_send.at[g], gather_recv.at[g, q, stage] if stage < 3 else swap_recv.at[g],
         )
 
     def gather_step(g, q, stage):
         if stage:
             for copy in gather_copies(g, q, stage - 1, True):
                 copy.wait_recv()
-        if stage < 4:
-            for copy in gather_copies(g, q, stage, False):
-                copy.start()
+        for copy in gather_copies(g, q, stage, False):
+            copy.start()
+
+    def gathered(g):
+        block = rows_all.at[g, :, :, :, 1 - c]
+        remote(block, block, gather_send.at[g], swap_recv.at[g], partner["c"]).wait_recv()
+
+    sent_blocks = sp_count * tp_count - 1
+
+    def wait_sent(send, lanes):
+        block = w_vmem.at[0 : sent_blocks * GROUP, 0:lanes]
+        remote(block, block, send, share_recv.at[0], partner["c"]).wait_send()
 
     group_rows = sp_count * tp_count * GROUP
     half_rows = group_rows // 2
@@ -548,7 +566,7 @@
     def reduce_order(q):
         return "c" + SPREAD[q][::-1]
 
-    def reduce_copies(g, q, stage):
+    def reduce_copies(g, q, stage, arriving=False):
         order, cols = reduce_order(q), span(q)
         at = {"z": every, "x": every, "y": every, "c": every}
         for axis in order[:stage]:
@@ -558,17 +576,17 @@
         def block(place):
             return parts.at[g, place["z"], place["x"], place["y"], place["c"], :, cols]
 
+        send, recv = reduce_send.at[g], reduce_recv.at[g, q, stage]
         if axis == "z":
-            copies = []
-            for d in range(1, z_count):
-                dst = got_mid.at[g, d - 1, :, :, cols] if stage == 2 else got_last.at[g, d - 1, :, cols]
-                copies.append(
-                    remote(
-                        block({**at, "z": lax.rem(z + d, z_count)}), dst,
-                        reduce_send.at[g, q, d - 1], reduce_recv.at[g, q, d - 1], z_peer(d),
-                    )
+            dst = got_mid.at[g, :, :, :, cols] if stage == 2 else got_last.at[g, :, :, cols]
+            if arriving:
+                return [remote(dst, dst, send, recv, partner["x"])]
+            return [
+                remote(
+                    block({**at, "z": lax.rem(z + d, z_count)}), dst.at[d - 1], send, recv, z_peer(d)
                 )
-            return copies
+                for d in range(1, z_count)
+            ]
         own = {"x": x, "y": y, "c": c}[axis]
         dst = (
             got_core.at[g, :, :, :, :, cols] if stage == 0
@@ -576,19 +594,19 @@
             else got_two.at[g, :, :, cols] if stage == 2
             else got_last.at[g, 0, :, cols]
         )
-        slot = z_count - 1 + "xyc".index(axis)
-        return [
-            remote(
-                block({**at, axis: 1 - own}), dst,
-                reduce_send.at[g, q, slot], reduce_recv.at[g, q, slot], partner[axis],
-            )
-        ]
+        return [remote(block({**at, axis: 1 - own}), dst, send, recv, partner[axis])]
+
+    def store(g, q):
+        here = slice(g * GROUP, (g + 1) * GROUP)
+        return pltpu.make_async_copy(
+            out_rows.at[here, span(q)], out_ref.at[here, span(q)], out_sem
+        )
 
     def f32(value):
         return value.astype(jnp.float32)
 
     def absorb_step(g, q, stage):
-        for copy in reduce_copies(g, q, stage):
+        for copy in reduce_copies(g, q, stage, True):
             copy.wait_recv()
         order = reduce_order(q)
         at, size = cuts[q]
@@ -618,8 +636,9 @@
             total = f32(parts[g, z, x, y, c, :, cols])
             for d in range(1, z_count if order[3] == "z" else 2):
                 total = total + f32(got_last[g, d - 1, :, cols])
-            here = pl.ds(pl.multiple_of(g * GROUP, GROUP), GROUP)
-            out_ref[here, cols] = (f32(res_ref[here, cols]) + total).astype(jnp.bfloat16)
+            here = slice(g * GROUP, (g + 1) * GROUP)
+            out_rows[here, cols] = (f32(res_ref[here, cols]) + total).astype(jnp.bfloat16)
+            store(g, q).start()
 
     def reduce_step(g, q, stage):
         if stage:
@@ -628,59 +647,54 @@
             for copy in reduce_copies(g, q, stage):
                 copy.start()
 
-    def at_lag(it, q, lag, step):
-        g = it + (q - lag) // chunks
-
-        @pl.when((g >= 0) & (g < groups))
-        def _():
-            step(g, (q - lag) % chunks)
-
-    last = groups * chunks - 1 + REDUCE_AT + REDUCE_LAG[4]
-    share_step(3)
-
-    @pl.loop(0, last // chunks + 1)
-    def _(it):
-        @pl.when(it == 2)
-        def _():
-            share_step(4)
-            for load in large[1:]:
-                load.wait()
-
-        for q in range(chunks):
-            for stage in (0, 1, 2, 3, 4):
-                at_lag(it, q, GATHER_LAG[stage], functools.partial(gather_step, stage=stage))
-            if q == chunks - 1:
-                at_lag(it, q, GATHER_LAG[4], lambda g, _: raise_half(g, 0))
-            if q == 0:
-                at_lag(it, q, GATHER_LAG[4] + 1, lambda g, _: raise_half(g, 1))
-            at_lag(it, q, REDUCE_AT, lower_chunk)
-            for stage in (0, 1, 2, 3, 4):
-                at_lag(it, q, REDUCE_AT + REDUCE_LAG[stage], functools.partial(reduce_step, stage=stage))
-
-    @pl.loop(1, sp_count - sp_me)
-    def _(d):
-        state_copy(sp_me, d).wait_send()
-
-    for d in range(1, tp_count):
-        mix_copy(lax.rem(tp_me + d, tp_count), tp_me, d).wait_send()
-    for stage in range(4):
-        for copy in share_copies(stage, False):
-            copy.wait_send()
-
-    @pl.loop(0, groups)
-    def _(g):
+    events = []
+
+    def plan(time, step, *args):
+        events.append((time, len(events), step, args))
+
+    def load_weights():
+        for load in large[1:]:
+            load.wait()
+
+        state_all.wait_send()
+        mix_all.wait_send()
+
+    for i, time in enumerate(SHARE_AT):
+        plan(time, share_step, i)
+    for g in range(groups):
+        ready = 0.0
         for q in range(chunks):
             for stage in range(4):
-                for copy in gather_copies(g, q, stage, False):
-                    copy.wait_send()
-                for copy in reduce_copies(g, q, stage):
-                    copy.wait_send()
+                plan(max(g * GATHER_PACE + GATHER_AT[q][stage], 0.0), gather_step, g, q, stage)
+            ready = max(ready, g * GATHER_PACE + GATHER_AT[q][4])
+        plan(ready, gathered, g)
+        if g == 0:
+            plan(ready, load_weights)
+        plan(ready, raise_half, g, 0)
+        plan(ready + RAISE_GAP, raise_half, g, 1)
+        begin = max(ready + 2 * RAISE_GAP, REDUCE_FROM + g * REDUCE_PACE)
+        for q in range(chunks):
+            plan(begin + REDUCE_AT[q][0], lower_chunk, g, q)
+            for stage in range(5):
+                plan(begin + REDUCE_AT[q][stage], reduce_step, g, q, stage)
+    for _, _, step, args in sorted(events, key=lambda event: event[:2]):
+        step(*args)
+
+    wait_sent(share_send, rows * LANES // GROUP)
+    for g in range(groups):
+        wait_sent(gather_send.at[g], width)
+        wait_sent(reduce_send.at[g], width)
+    pltpu.make_async_copy(out_rows, out_ref, out_sem).wait()
 
 
 def column_cuts(width):
-    tiles = width // LANES
-    edges = [tiles * share // 16 * LANES for share in (0, 5, 10, 13, 16)]
-    return [(edges[i], edges[i + 1] - edges[i]) for i in range(4)]
+    tiles, total = width // LANES, sum(part for _, part in PIECES)
+    cuts, passed = [], 0
+    for _, part in PIECES:
+        first, end = (tiles * n // total * LANES for n in (passed, passed + part))
+        cuts.append((first, end - first))
+        passed += part
+    return cuts
 
 
 def layer_rows(
@@ -696,10 +710,8 @@
     group_rows = sp_count * tp_count * GROUP
     cuts = column_cuts(width)
     hbm = pl.BlockSpec(memory_space=pl.ANY)
-    vmem = pl.BlockSpec(memory_space=pltpu.VMEM)
     bf16, f32 = jnp.bfloat16, jnp.float32
     dma = pltpu.SemaphoreType.DMA
-    ways = z_count + 2
     operands = (
         queries, key_rows, value_rows, out_gate, decay_logit, head_gain.reshape(1, -1), w_out,
         ffn_gain.reshape(-1, LANES), routing.T, route_weight.T, residual_in,
@@ -713,7 +725,7 @@
         functools.partial(layer_kernel, sp_count, tp_count, cuts),
         out_shape=jax.ShapeDtypeStruct((rows, width), bf16),
         in_specs=[hbm] * len(operands),
-        out_specs=vmem,
+        out_specs=hbm,
         scratch_shapes=[
             *(like(operands[i]) for i in (0, 1, 2, 3, 4, 5, 7, 8, 9, 10)),
             pltpu.VMEM((sp_count, DV + 16, key_lanes), bf16),
@@ -734,18 +746,21 @@
             pltpu.VMEM((groups, z_count, GROUP, width), bf16),
             pltpu.VMEM((groups, z_count - 1, 2, GROUP, width), bf16),
             pltpu.VMEM((groups, z_count - 1, GROUP, width), bf16),
+            pltpu.VMEM((rows, width), bf16),
             dma((10,)),
             dma((4,)),
-            dma((sp_count,)),
-            dma((sp_count,)),
-            dma((tp_count,)),
-            dma((tp_count,)),
-            dma((ways,)),
-            dma((ways,)),
-            dma((groups, 4, ways)),
-            dma((groups, 4, ways)),
-            dma((groups, 4, ways)),
-            dma((groups, 4, ways)),
+            dma,
+            dma,
+            dma,
+            dma,
+            dma,
+            dma((4,)),
+            dma((groups,)),
+            dma((groups, len(cuts), 3)),
+            dma((groups,)),
+            dma((groups,)),
+            dma((groups, len(cuts), 4)),
+            dma,
         ],
         compiler_params=pltpu.CompilerParams(
             collective_id=1, has_side_effects=True, vmem_limit_bytes=62 << 20
@@ -800,6 +815,8 @@
     if (
         capacity >= quarter and experts <= LANES // 2 and experts % 4 == 0
         and tp_count == 4 and quarter % GROUP == 0
+        and w_out.shape[0] >= (experts * tp_count - 1) * GROUP and model_width % (16 * LANES) == 0
+        and quarter * LANES // GROUP <= model_width
     ):
         return layer_rows(
             queries, key_rows, value_rows, out_gate, decay_logit, head_gain, w_out,

time: 117 us -> 104 us (0.89)
  Pallas kernels: 115 us -> 103 us
    pallas_call x1, Pallas kernels: 115 us -> 103 us  [layer_rows(): pl.pallas_call(functools.partial(layer_kernel, sp_count, tp_count, cuts),...]
where the time goes in v2:
time: 104 us
  Pallas kernels  103 us (99%)
  local copies, waits for them, and re-layouts  1.67 us (2%)
    pallas_call x1, Pallas kernels, layer_rows(): pl.pallas_call(functools.partial(layer_kernel, sp_count, tp_count, cuts),...  103 us

profile of v2, /device:TPU:0, one launch (start us, length us, event | category | flops | bytes accessed | tf_op | source)
XLA Modules:
  0.0 104.3 jit_solution(15704278988098146221)
XLA Ops:
  0.0 102.7 %layer_rows.1 = bf16[64,2048]{1,0:T(8,128)(2,1)} custom-call(bf16[256,128]{1,0:T(8,128)(2,1)} %q_hbm.1, bf16[256,128]{1,0:T(8,128)(2,1)} %k_hbm.1, bf16[256,256]{1,0:T(8,128)(2,1)} %v_hbm.1, bf16[256,256]{1,0:T(8,128)(2,1)} %gate_hbm.1, f32[256,128]{1,0:T(8,128)} %decay_hbm.1, bf16[1,128]{1,0:T(2,128)(2,1)} %bitcast.13, bf16[1024,2048]{1,0:T(8,128)(2,1)} %w_out_hbm.1, ...), custom_call_target="tpu_custom_call" | custom-call | tf_op jit(solution)/shard_map/layer_rows/pallas_call | solution.py:724
  102.7 1.7 %copy.16 = bf16[64,2048]{1,0:T(8,128)(2,1)} copy(bf16[64,2048]{1,0:T(8,128)(2,1)} %layer_rows.1) | data formatting | bytes 524288

commit v3 on v2

--- a/solution.py
+++ b/solution.py
@@ -272,9 +272,9 @@
     out_ref,
     q_ref, k_ref, v_ref, gate_ref, decay_ref, head_gain_ref, ffn_gain_ref,
     routing_ref, weight_ref, res_ref,
-    states, attended, opened, mixed, mixed_in, w_vmem,
+    states, passed, attended, opened, mixed, mixed_in, w_vmem,
     rows_all, share_all, gate_w, up_w, down_w, hidden, parts, got_core, got_one, got_two, got_mid, got_last, out_rows,
-    in_sem, w_sem, state_send, state_recv, mix_send, mix_recv,
+    in_sem, w_sem, state_send, state_recv, passed_send, passed_recv, mix_send, mix_recv,
     share_send, share_recv, gather_send, gather_recv, swap_recv, reduce_send, reduce_recv, out_sem,
 ):
     sp_me, tp_me = lax.axis_index("sp"), lax.axis_index("tp")
@@ -362,14 +362,8 @@
     state = jnp.zeros((DV, key_lanes), jnp.float32)
     for h in range(head_count):
         state = jnp.where(lane_head == h, wide[h * DV : (h + 1) * DV, :], state)
-    passing = jnp.exp(ending)
-    passing_hi = passing.astype(jnp.bfloat16).astype(jnp.float32)
-    tail_row = lax.broadcasted_iota(jnp.int32, (16, key_lanes), 0)
-    tail = jnp.where(
-        tail_row == 0, passing_hi, jnp.where(tail_row == 1, passing - passing_hi, 0.0)
-    )
-    states[sp_me, 0:DV, :] = state.astype(jnp.bfloat16)
-    states[sp_me, DV : DV + 16, :] = tail.astype(jnp.bfloat16)
+    states[sp_me] = state.astype(jnp.bfloat16)
+    passed[sp_me] = jnp.exp(ending)
 
     pl.semaphore_wait(barrier, sp_count + tp_count - 2)
 
@@ -379,8 +373,15 @@
             {"sp": lax.rem(sp_me + d, sp_count)},
         )
 
+    def passed_copy(slot, d):
+        return remote(
+            passed.at[slot], passed.at[slot], passed_send, passed_recv,
+            {"sp": lax.rem(sp_me + d, sp_count)},
+        )
+
     @pl.loop(1, sp_count)
     def _(d):
+        passed_copy(sp_me, d).start()
         state_copy(sp_me, d).start()
 
     lane = lax.broadcasted_iota(jnp.int32, (LANES, tokens), 0)
@@ -454,11 +455,12 @@
     others = states.at[0 : sp_count - 1]
     state_all = remote(others, others, state_send, state_recv, partner["x"])
     state_all.wait_recv()
+    others = passed.at[0 : sp_count - 1]
+    passed_all = remote(others, others, passed_send, passed_recv, partner["x"])
+    passed_all.wait_recv()
 
     def absorb(j, incoming):
-        decay = states[j, DV : DV + 16, :].astype(jnp.float32)
-        total = decay[0:1, :] + decay[1:2, :]
-        return total * incoming + states[j, 0:DV, :].astype(jnp.float32)
+        return passed[j] * incoming + states[j].astype(jnp.float32)
 
     incoming = lax.fori_loop(
         0, sp_me, absorb, jnp.zeros((DV, key_lanes), jnp.float32)
@@ -471,14 +473,15 @@
         scale = lax.rsqrt(jnp.mean(head * head, axis=-1, keepdims=True) + NORM_EPS)
         mixed[:, cols] = (head * scale * opened[:, cols]).astype(jnp.bfloat16)
 
-    def mix_copy(block, slot, d):
+    def mix_copy(block, i):
         return remote(
-            mixed.at[pl.ds(pl.multiple_of(block * rows, rows), rows)], mixed_in.at[slot],
-            mix_send, mix_recv, {"tp": lax.rem(tp_me + d, tp_count)},
-        )
-
-    for d in range(1, tp_count):
-        mix_copy(lax.rem(tp_me + d, tp_count), tp_count - d - 1, d).start()
+            mixed.at[pl.ds(pl.multiple_of(block * rows, rows), rows)], mixed_in.at[i],
+            mix_send, mix_recv.at[i], {"tp": block},
+        )
+
+    others = ((y, 1 - c), (1 - y, c), (1 - y, 1 - c))
+    for i, (yy, cc) in enumerate(others):
+        mix_copy(yy * 2 + cc, i).start()
     large[0].wait()
 
     def w_rows(j):
@@ -489,14 +492,12 @@
         w_rows(tp_me),
         preferred_element_type=jnp.float32,
     )
-    incoming_mix = mixed_in.at[0 : tp_count - 1]
-    mix_all = remote(incoming_mix, incoming_mix, mix_send, mix_recv, partner["c"])
-    mix_all.wait_recv()
-    for d in range(1, tp_count):
-        slot = lax.rem(tp_me + d, tp_count)
+    for i, (yy, cc) in enumerate(others):
+        mix_copy(yy * 2 + cc, i).wait_recv()
         projected = projected + jnp.dot(
-            mixed_in[d - 1], w_rows(slot), preferred_element_type=jnp.float32
-        )
+            mixed_in[i], w_rows(yy * 2 + cc), preferred_element_type=jnp.float32
+        )
+    mix_all = remote(mixed_in, mixed_in, mix_send, mix_recv.at[0], partner["c"])
     residual = (res_ref[...].astype(jnp.float32) + projected).astype(jnp.bfloat16)
     res_ref[...] = residual
     wide_res = residual.astype(jnp.float32)
@@ -657,6 +658,7 @@
             load.wait()
 
         state_all.wait_send()
+        passed_all.wait_send()
         mix_all.wait_send()
 
     for i, time in enumerate(SHARE_AT):
@@ -728,11 +730,12 @@
         out_specs=hbm,
         scratch_shapes=[
             *(like(operands[i]) for i in (0, 1, 2, 3, 4, 5, 7, 8, 9, 10)),
-            pltpu.VMEM((sp_count, DV + 16, key_lanes), bf16),
+            pltpu.VMEM((sp_count, DV, key_lanes), bf16),
+            pltpu.VMEM((sp_count, 1, key_lanes), f32),
             pltpu.VMEM((tokens, value_lanes), f32),
             pltpu.VMEM((tokens, value_lanes), f32),
             pltpu.VMEM((tokens, value_lanes), bf16),
-            pltpu.VMEM((tp_count, rows, value_lanes), bf16),
+            pltpu.VMEM((tp_count - 1, rows, value_lanes), bf16),
             like(w_out),
             pltpu.VMEM((groups, z_count, 2, 2, 2, GROUP, width), bf16),
             pltpu.VMEM((z_count, 2, 2, 2, rows, LANES), bf16),
@@ -753,6 +756,8 @@
             dma,
             dma,
             dma,
+            dma,
+            dma((tp_count - 1,)),
             dma,
             dma((4,)),
             dma((groups,)),

time: 104 us -> 102 us (0.981)
  Pallas kernels: 103 us -> 100 us
    pallas_call x1, Pallas kernels: 103 us -> 100 us  [layer_rows(): pl.pallas_call(functools.partial(layer_kernel, sp_count, tp_count, cuts),...]
where the time goes in v3:
time: 102 us
  Pallas kernels  100 us (98%)
  local copies, waits for them, and re-layouts  1.67 us (2%)
    pallas_call x1, Pallas kernels, layer_rows(): pl.pallas_call(functools.partial(layer_kernel, sp_count, tp_count, cuts),...  100 us

profile of v3, /device:TPU:0, one launch (start us, length us, event | category | flops | bytes accessed | tf_op | source)
XLA Modules:
  0.0 102.1 jit_solution(6526230552767398736)
XLA Ops:
  0.0 100.4 %layer_rows.1 = bf16[64,2048]{1,0:T(8,128)(2,1)} custom-call(bf16[256,128]{1,0:T(8,128)(2,1)} %q_hbm.1, bf16[256,128]{1,0:T(8,128)(2,1)} %k_hbm.1, bf16[256,256]{1,0:T(8,128)(2,1)} %v_hbm.1, bf16[256,256]{1,0:T(8,128)(2,1)} %gate_hbm.1, f32[256,128]{1,0:T(8,128)} %decay_hbm.1, bf16[1,128]{1,0:T(2,128)(2,1)} %bitcast.13, bf16[1024,2048]{1,0:T(8,128)(2,1)} %w_out_hbm.1, ...), custom_call_target="tpu_custom_call" | custom-call | tf_op jit(solution)/shard_map/layer_rows/pallas_call | solution.py:726
  100.4 1.7 %copy.16 = bf16[64,2048]{1,0:T(8,128)(2,1)} copy(bf16[64,2048]{1,0:T(8,128)(2,1)} %layer_rows.1) | data formatting | bytes 524288
